TPU v7x, 32 devices: a whole 2x2x4 slice. The times are simulated.
32 devices in a mesh: grp: 2 (over y), sp: 4 (over z), tp: 4 (over x, core).
Axes of the slice: x: 2, y: 2, z: 4, core: 2. Of those that a mesh axis runs over, the one named last changes fastest.
Arguments:
- stream: bfloat16 [3072, 4096], P(('grp', 'sp'), 'tp'), parts along dimension 0, may hold values from -6 to 6
- norm_gain: bfloat16 [2, 4096], replicated, may hold values from 0.099609375 to 1.8984375
- w_signal: bfloat16 [2, 4096, 1024], P(None, 'sp', 'tp'), may hold values from -0.09375 to 0.09375
- w_gate: bfloat16 [2, 4096, 1024], P(None, 'sp', 'tp'), may hold values from -0.09375 to 0.09375
- conv_taps: bfloat16 [2, 31, 1024], P(None, None, 'tp'), may hold values from -4 to 4
- conv_bias: bfloat16 [2, 1024], P(None, 'tp'), may hold values from -3 to 3
- ln_gain: bfloat16 [2, 1024], P(None, 'tp'), may hold values from 0.099609375 to 1.8984375
- ln_shift: bfloat16 [2, 1024], P(None, 'tp'), may hold values from -3 to 3
- w_out: bfloat16 [2, 1024, 4096], P(None, 'sp', 'tp'), may hold values from -0.375 to 0.375
Outputs:
- mixed_stream: bfloat16 [3072, 4096], P(('grp', 'sp'), 'tp'), parts along dimension 0
There are 2 independent parts, one for each index of `grp`. A program takes and returns all parts, laid end to end along the dimension named above; an argument that names none is the same for every part. Nothing has to cross between parts.
All inputs are finite; a program needn't handle non-finite values.
Results may differ from a plain program's by a relative error of at most 0.01.
Values may be sent and summed in bfloat16 or wider, within the bound.
A program may use at most 64 MiB of HBM per device.

v0:
```python
import jax
import jax.numpy as jnp
from jax import lax
from jax.sharding import PartitionSpec as P

C = 1024


EPS = 1e-05


def shifted(value, axis, steps):
    count = lax.axis_size(axis)
    initial, last = (max(0, -steps), min(count, count - steps))
    return lax.ppermute(value, axis, [(source, source + steps) for source in range(initial, last)])


def product(left, right):
    return jnp.dot(left, right, preferred_element_type=jnp.float32)


def shards(stream, norm_gain, w_signal, w_gate, conv_taps, conv_bias, ln_gain, ln_shift, w_out):
    fringe_rows = conv_taps.shape[1] - 1
    own_rows = stream.shape[0]
    layer_count = w_signal.shape[0]
    local_channels = w_signal.shape[2]
    whole_signal, whole_gate, whole_out = (
        lax.all_gather(w_signal, "sp", axis=1, tiled=True),
        lax.all_gather(w_gate, "sp", axis=1, tiled=True),
        lax.all_gather(w_out, "sp", axis=1, tiled=True),
    )
    current = stream
    for layer_index in range(layer_count):
        features = lax.all_gather(current, "tp", axis=1, tiled=True)
        widened = features.astype(jnp.float32)
        normed = (
            widened
            * lax.rsqrt(jnp.mean(widened * widened, axis=-1, keepdims=True) + EPS)
            * norm_gain[layer_index].astype(jnp.float32)
        ).astype(jnp.bfloat16)
        signal = product(normed, whole_signal[layer_index])
        gate_pre = product(normed, whole_gate[layer_index])
        blended = (signal * jax.nn.sigmoid(gate_pre)).astype(jnp.bfloat16)
        earlier = shifted(blended[own_rows - fringe_rows :], "sp", 1)
        padded = jnp.concatenate([earlier, blended], axis=0)
        length = padded.shape[0] - fringe_rows
        filtered = jnp.zeros((length, local_channels), jnp.float32) + conv_bias[layer_index].astype(
            jnp.float32
        )
        tap_rows = conv_taps[layer_index].astype(jnp.float32)
        for tap_index in range(fringe_rows + 1):
            filtered = filtered + tap_rows[tap_index] * padded[
                tap_index : tap_index + length
            ].astype(jnp.float32)
        totals = lax.psum((jnp.sum(filtered, axis=-1), jnp.sum(filtered * filtered, axis=-1)), "tp")
        average = totals[0][:, None] / C
        spread = totals[1][:, None] / C - average * average
        scaled = (filtered - average) * lax.rsqrt(spread + EPS) * ln_gain[layer_index].astype(
            jnp.float32
        ) + ln_shift[layer_index].astype(jnp.float32)
        activated = jax.nn.silu(scaled).astype(jnp.bfloat16)
        channels = lax.all_gather(activated, "tp", axis=1, tiled=True)
        update = product(channels, whole_out[layer_index])
        current = (current.astype(jnp.float32) + update).astype(jnp.bfloat16)
    return current


def solution(mesh):
    return jax.shard_map(
        shards,
        mesh=mesh,
        in_specs=(
            P(("grp", "sp"), "tp"),
            P(),
            P(None, "sp", "tp"),
            P(None, "sp", "tp"),
            P(None, None, "tp"),
            P(None, "tp"),
            P(None, "tp"),
            P(None, "tp"),
            P(None, "sp", "tp"),
        ),
        out_specs=P(("grp", "sp"), "tp"),
        check_vma=False,
    )
```

profile of v0, /device:TPU:0, one launch (start us, length us, event | category | flops | bytes accessed | tf_op | source)
XLA Modules:
  0.0 354.0 jit_solution(9451302702197944775)
XLA Ops:
  6.5 0.0 all-gather.6.cloned.1.call-start
  6.5 0.7 all-gather.6.cloned.1.call-update
  7.3 0.0 all-gather.10.cloned.1.call-start
  7.3 0.7 all-gather.10.cloned.1.call-update
  8.0 0.0 all-gather.8.cloned.1.call-start
  8.1 0.7 all-gather.8.cloned.1.call-update
  8.7 0.0 all-gather.12.cloned.1.call-start
  8.8 0.5 all-gather.12.cloned.1.call-update
  9.3 0.0 all-gather.14.cloned.1.call-start
  9.4 0.8 slice_convert_fusion.6
  10.1 0.8 slice_convert_fusion.5
  10.9 0.9 slice_convert_fusion
  11.8 0.8 slice_convert_fusion.2
  12.6 27.5 %all-gather.6.cloned.1.call-done = bf16[384,4096]{1,0:T(8,128)(2,1)} async-done(((bf16[384,1024]{1,0:T(8,128)(2,1)}), bf16[384,4096]{1,0:T(8,128)(2,1)}) %all-gather.6.cloned.1.call-update) | async-done | bytes 3145744 | tf_op jit(solution)/shard_map/all_gather | solution.py:34
  40.2 2.6 fusion
  42.7 79.8 %all-gather.10.cloned.1.call-done = bf16[2,4096,256]{2,1,0:T(8,128)(2,1)} async-done(((bf16[2,1024,256]{2,1,0:T(8,128)(2,1)}), bf16[2,4096,256]{2,1,0:T(8,128)(2,1)}) %all-gather.10.cloned.1.call-update) | async-done | bytes 4194320 | tf_op jit(solution)/shard_map/all_gather | solution.py:29
  122.5 0.0 copy-start
  122.5 4.5 %fusion.21 = f32[384,256]{1,0:T(8,128)} fusion(bf16[2,4096,256]{2,1,0:T(8,128)(2,1)} %all-gather.10.cloned.1.call-done, bf16[384,4096]{1,0:T(8,128)(2,1)} %all-gather.6.cloned.1.call-done, f32[4096]{0:T(1024)S(1)} %bitcast.120, f32[384]{0:T(512)S(1)} %add_rsqrt_fusion.3), kind=kOutput, calls=%fused_computation.91 | convolution fusion | flops 811892736 | bytes 5654016 | tf_op jit(solution)/shard_map/dot_general | solution.py:19
  127.0 0.0 copy-start.3
  127.0 76.4 %all-gather.8.cloned.1.call-done = bf16[2,4096,256]{2,1,0:T(8,128)(2,1)} async-done(((bf16[2,1024,256]{2,1,0:T(8,128)(2,1)}), bf16[2,4096,256]{2,1,0:T(8,128)(2,1)}) %all-gather.8.cloned.1.call-update) | async-done | bytes 4194320 | tf_op jit(solution)/shard_map/all_gather | solution.py:28
  203.3 0.0 copy-done
  203.3 2.8 fusion.23
  206.1 1.3 collective-permute-start
  207.4 0.0 copy-done.3
  207.4 1.4 collective-permute-done
  208.8 1.9 fusion.87
  210.7 5.9 %all-reduce.1 = (f32[384]{0:T(512)S(1)}, f32[384]{0:T(512)S(1)}) all-reduce(f32[384]{0:T(512)S(1)} %get-tuple-element.8, f32[384]{0:T(512)S(1)} %get-tuple-element.7), channel_id=1, replica_groups=mesh['grp'=2,'sp'=4,'tp'=4] {'tp'}, use_global_device_ids=true, to_apply=%region_4.0 | all-reduce | flops 768 | bytes 6144 | tf_op jit(solution)/shard_map/psum | solution.py:55
  216.6 0.2 multiply_convert_fusion.1
  216.8 8.8 %all_gather.24 = bf16[384,1024]{1,0:T(8,128)(2,1)S(1)} all-gather(bf16[384,256]{1,0:T(8,128)(2,1)S(1)} %multiply_convert_fusion.1), channel_id=1, replica_groups=mesh['grp'=2,'sp'=4,'tp'=4] {'tp'}, dimensions={1}, use_global_device_ids=true | all-gather | bytes 983040 | tf_op jit(solution)/shard_map/all_gather | solution.py:62
  225.6 58.4 %all-gather.12.cloned.1.call-done = bf16[2,1024,1024]{2,1,0:T(8,128)(2,1)} async-done(((bf16[2,256,1024]{2,1,0:T(8,128)(2,1)}), bf16[2,1024,1024]{2,1,0:T(8,128)(2,1)}) %all-gather.12.cloned.1.call-update) | async-done | bytes 4194320 | tf_op jit(solution)/shard_map/all_gather | solution.py:30
  284.0 3.6 %add_convert_fusion.1 = bf16[384,1024]{1,0:T(8,128)(2,1)} fusion(bf16[384,1024]{1,0:T(8,128)(2,1)} %param.9, bf16[384,1024]{1,0:T(8,128)(2,1)S(1)} %all_gather.24, bf16[2,1024,1024]{2,1,0:T(8,128)(2,1)} %all-gather.12.cloned.1.call-done), kind=kOutput, calls=%fused_computation.81 | convolution fusion | flops 806486016 | bytes 4456448 | tf_op jit(solution)/shard_map/dot_general | solution.py:19
  287.6 0.0 all-gather.14.cloned.1.call-update
  287.7 27.1 %all-gather.14.cloned.1.call-done = bf16[384,4096]{1,0:T(8,128)(2,1)} async-done(((bf16[384,1024]{1,0:T(8,128)(2,1)}), bf16[384,4096]{1,0:T(8,128)(2,1)}) %all-gather.14.cloned.1.call-update) | async-done | bytes 3145744 | tf_op jit(solution)/shard_map/all_gather | solution.py:34
  314.8 2.6 fusion.3
  317.4 0.0 copy-start.1
  317.4 0.0 copy-start.4
  317.4 3.7 %fusion.19 = f32[384,256]{1,0:T(8,128)S(1)} fusion(bf16[2,4096,256]{2,1,0:T(8,128)(2,1)} %all-gather.10.cloned.1.call-done, bf16[384,4096]{1,0:T(8,128)(2,1)} %all-gather.14.cloned.1.call-done, f32[4096]{0:T(1024)S(1)} %bitcast.118, f32[384]{0:T(512)S(1)} %add_rsqrt_fusion.1), kind=kOutput, calls=%fused_computation.89 | convolution fusion | flops 811892736 | bytes 5654016 | tf_op jit(solution)/shard_map/dot_general | solution.py:19
  321.2 0.0 copy-done.1
  321.2 1.0 copy-done.4
  322.1 0.0 copy-start.2
  322.1 1.0 fusion.22
  323.2 3.4 collective-permute-start.1
  326.6 1.4 collective-permute-done.1
  328.0 1.9 fusion.86
  329.9 5.9 %all-reduce = (f32[384]{0:T(512)S(1)}, f32[384]{0:T(512)S(1)}) all-reduce(f32[384]{0:T(512)S(1)} %get-tuple-element.6, f32[384]{0:T(512)S(1)} %get-tuple-element.5), channel_id=1, replica_groups=mesh['grp'=2,'sp'=4,'tp'=4] {'tp'}, use_global_device_ids=true, to_apply=%region_9.10 | all-reduce | flops 768 | bytes 6144 | tf_op jit(solution)/shard_map/psum | solution.py:55
  335.9 0.2 multiply_convert_fusion
  336.1 7.9 %all_gather.27 = bf16[384,1024]{1,0:T(8,128)(2,1)S(1)} all-gather(bf16[384,256]{1,0:T(8,128)(2,1)S(1)} %multiply_convert_fusion), channel_id=1, replica_groups=mesh['grp'=2,'sp'=4,'tp'=4] {'tp'}, dimensions={1}, use_global_device_ids=true | all-gather | bytes 983040 | tf_op jit(solution)/shard_map/all_gather | solution.py:62
  344.0 0.0 copy-done.2
  344.1 3.5 add_convert_fusion
  (11 shorter events, 0.1 us)
Async XLA Ops:
  6.5 33.6 %all-gather.6.cloned.1.call-start = ((), (), s32[]{:S(2)}) async-start(), calls=%async_computation | async-start | bytes 3932160 | tf_op jit(solution)/shard_map/all_gather | solution.py:34
  7.3 115.2 %all-gather.10.cloned.1.call-start = ((), (), s32[]{:S(2)}) async-start(), calls=%async_computation.2 | async-start | bytes 5242880 | tf_op jit(solution)/shard_map/all_gather | solution.py:29
  8.0 195.3 %all-gather.8.cloned.1.call-start = ((), (), s32[]{:S(2)}) async-start(), calls=%async_computation.1 | async-start | bytes 5242880 | tf_op jit(solution)/shard_map/all_gather | solution.py:28
  8.7 275.3 %all-gather.12.cloned.1.call-start = ((), (), s32[]{:S(2)}) async-start(), calls=%async_computation.3 | async-start | bytes 5242880 | tf_op jit(solution)/shard_map/all_gather | solution.py:30
  9.3 305.5 %all-gather.14.cloned.1.call-start = ((), (), s32[]{:S(2)}) async-start(), calls=%async_computation.4 | async-start | bytes 3932160 | tf_op jit(solution)/shard_map/all_gather | solution.py:34
  122.5 80.8 %copy-start = (bf16[384,4096]{1,0:T(8,128)(2,1)S(1)}, bf16[384,4096]{1,0:T(8,128)(2,1)}, u32[]{:S(2)}) copy-start(bf16[384,4096]{1,0:T(8,128)(2,1)} %all-gather.6.cloned.1.call-done) | copy-start | bytes 9437188
  127.0 80.4 %copy-start.3 = (bf16[2,256]{1,0:T(2,128)(2,1)S(1)}, bf16[2,256]{1,0:T(2,128)(2,1)}, u32[]{:S(2)}) copy-start(bf16[2,256]{1,0:T(2,128)(2,1)} %param.16) | copy-start | bytes 3076
  206.1 2.7 collective-permute-start
  317.4 3.8 %copy-start.1 = (bf16[384,4096]{1,0:T(8,128)(2,1)S(1)}, bf16[384,4096]{1,0:T(8,128)(2,1)}, u32[]{:S(2)}) copy-start(bf16[384,4096]{1,0:T(8,128)(2,1)} %all-gather.14.cloned.1.call-done) | copy-start | bytes 9437188
  317.4 4.7 %copy-start.4 = (bf16[2,4096,256]{2,1,0:T(8,128)(2,1)S(1)}, bf16[2,4096,256]{2,1,0:T(8,128)(2,1)}, u32[]{:S(2)}) copy-start(bf16[2,4096,256]{2,1,0:T(8,128)(2,1)} %all-gather.8.cloned.1.call-done) | copy-start | bytes 12582916
  322.1 21.9 %copy-start.2 = (bf16[384,1024]{1,0:T(8,128)(2,1)S(1)}, bf16[384,1024]{1,0:T(8,128)(2,1)}, u32[]{:S(2)}) copy-start(bf16[384,1024]{1,0:T(8,128)(2,1)} %add_convert_fusion.1) | copy-start | bytes 2359300
  323.2 4.8 %collective-permute-start.1 = (bf16[30,256]{1,0:T(8,128)(2,1)S(1)}, bf16[30,256]{1,0:T(8,128)(2,1)S(1)}, u32[]{:S(2)}, u32[]{:S(2)}) collective-permute-start(bf16[30,256]{1,0:T(8,128)(2,1)S(1)} %slice.718), channel_id=1, source_target_pairs={{0,4},{4,8},{8,12},{1,5},{5,9},{9,13},{2,6},{6,10},{10,14},{3,7},{... | collective-permute-start | bytes 46088 | tf_op jit(solution)/shard_map/ppermute | solution.py:15
Sparse Core Ops, SparseCore 0:
  8.9 31.2 all-gather.5
  41.7 80.7 all-gather.9
  124.1 79.2 all-gather.7
  204.8 79.2 all-gather.11
  287.8 26.9 all-gather.13
where the time goes:
time: 355 us; the launch traced here: 354 us
  waiting for transfers between devices  275 us (77%)
  blocking collectives  28.5 us (8%)
  matrix products  19.1 us (5%)
  between operations  13.3 us (4%)
  other arithmetic  12.7 us (4%)
  starting transfers between devices  4.83 us (1%)
    all_gather x1, waiting for transfers between devices, shards(): lax.all_gather(w_gate, 'sp', axis=1, tiled=True)  79.8 us
    all_gather x1, waiting for transfers between devices, shards(): lax.all_gather(w_signal, 'sp', axis=1, tiled=True)  76.4 us
    all_gather x1, waiting for transfers between devices, shards(): lax.all_gather(w_out, 'sp', axis=1, tiled=True)  58.4 us
    all_gather x2, waiting for transfers between devices, shards(): features = lax.all_gather(current, 'tp', axis=1, tiled=True)  54.7 us
    dot_general x6, matrix products, product(): return jnp.dot(left, right, preferred_element_type=jnp.float32)  19.1 us
    all_gather x2, blocking collectives, shards(): channels = lax.all_gather(activated, 'tp', axis=1, tiled=True)  16.7 us
    psum x2, blocking collectives, shards(): lax.psum((jnp.sum(filtered, axis=-1), jnp.sum(filtered * filtered, axis=-...  11.8 us
  transfers between devices with their start and end apart: 7, of which 7 were waited for; matrix products, arithmetic and copies ran while one was open for 4% of the time, Pallas kernels for 0%

commit v1 on v0

v1 whole, which is shorter than its diff:
```python
import functools

import jax
import jax.numpy as jnp
from jax import lax
from jax.experimental import pallas as pl
from jax.experimental.pallas import tpu as pltpu
from jax.sharding import PartitionSpec as P

MESH = pl.DeviceIdType.MESH
EPS = 1e-05
F32 = jnp.float32
BF16 = jnp.bfloat16
SIG, GATE, OUT = 0, 1, 2
CHUNK = 32


def sigmoid(v):
    return 1.0 / (1.0 + jnp.exp(-v))


def kernel(
    sizes,
    stream, gain, w_signal, w_gate, taps, bias, ln_gain, ln_shift, w_out,
    result,
    sig_all, gate_all, out_all, feats, scaled_feats, inv, acc_sig, acc_gate,
    tail, halo, padded, filt, stat_cols, stat_rows, acts,
    load_sem, stream_sem, z_send, z_recv, y_send, y_recv,
    cross_send, cross_recv, core_send, core_recv,
    halo_send, halo_recv, stat_send, stat_recv,
):
    groups, sp, tp, layers, rows, kernel_taps, hp, width, channels = sizes
    g, s, t = lax.axis_index("grp"), lax.axis_index("sp"), lax.axis_index("tp")
    chips = tp // 2
    core, chip = lax.rem(t, 2), lax.div(t, 2)
    mate = t + 1 - 2 * core
    share = sp // tp
    banks = (sig_all, gate_all, out_all)
    held = (w_signal, w_gate, w_out)

    def load(l, k):
        return pltpu.make_async_copy(held[k].at[l], banks[k].at[l, s], load_sem.at[l, k])

    own_stream = pltpu.make_async_copy(stream, feats.at[0, t], stream_sem)
    own_stream.start()
    for l in range(layers):
        for k in range(3):
            load(l, k).start()

    barrier = pltpu.get_barrier_semaphore()

    def greet(where):
        pl.semaphore_signal(barrier, inc=1, device_id=where, device_id_type=MESH)

    @pl.when(s > 0)
    def _():
        greet({"sp": s - 1})

    @pl.when(s < sp - 1)
    def _():
        greet({"sp": s + 1})

    for i in range(1, groups):
        greet({"grp": lax.rem(g + i, groups)})
    for i in range(1, tp):
        greet({"tp": lax.rem(t + i, tp)})
    pl.semaphore_wait(
        barrier,
        jnp.where(s > 0, 1, 0) + jnp.where(s < sp - 1, 1, 0) + (groups - 1 + tp - 1),
    )

    def z_copy(l, k, shard, way):
        ref = banks[k].at[l, shard, g]
        return pltpu.make_async_remote_copy(
            src_ref=ref, dst_ref=ref,
            send_sem=z_send.at[l, k, way, shard], recv_sem=z_recv.at[l, k, shard],
            device_id={"sp": s + 1 if way == 0 else s - 1}, device_id_type=MESH,
        )

    def y_copy(l, k, shard):
        ref = banks[k].at[l, shard, g]
        return pltpu.make_async_remote_copy(
            src_ref=ref, dst_ref=ref,
            send_sem=y_send.at[l, k, shard], recv_sem=y_recv.at[l, k, shard],
            device_id={"grp": 1 - g}, device_id_type=MESH,
        )

    def own(l, k, done=False):
        if not done:
            load(l, k).wait()
        for way, there in ((0, s < sp - 1), (1, s > 0)):
            @pl.when(there)
            def _(way=way):
                copy = z_copy(l, k, s, way)
                copy.wait_send() if done else copy.start()

    def sides(d):
        return (
            (0, s - 1 - d, s - 1 - d >= 0, s < sp - 1),
            (1, s + 1 + d, s + 1 + d <= sp - 1, s > 0),
        )

    def relay(l, k, d, done=False):
        for way, shard, here, onward in sides(d):
            @pl.when(here)
            def _(way=way, shard=shard, onward=onward):
                if not done:
                    z_copy(l, k, shard, way).wait_recv()

                @pl.when(onward)
                def _():
                    copy = z_copy(l, k, shard, way)
                    copy.wait_send() if done else copy.start()

                copy = y_copy(l, k, shard)
                copy.wait_send() if done else copy.start()

    def other_half(l, k, d):
        for _, shard, here, _ in sides(d):
            @pl.when(here)
            def _(shard=shard):
                y_copy(l, k, shard).wait_recv()

    def cross_copy(buf, n, block, i):
        ref = buf.at[block]
        return pltpu.make_async_remote_copy(
            src_ref=ref, dst_ref=ref,
            send_sem=cross_send.at[n, i], recv_sem=cross_recv.at[n, block],
            device_id={"tp": lax.rem(chip + i, chips) * 2 + core}, device_id_type=MESH,
        )

    def core_copy(buf, n, block):
        ref = buf.at[block]
        return pltpu.make_async_remote_copy(
            src_ref=ref, dst_ref=ref,
            send_sem=core_send.at[n, block], recv_sem=core_recv.at[n, block],
            device_id={"tp": mate}, device_id_type=MESH,
        )

    def spread_start(buf, n):
        for i in range(1, chips):
            cross_copy(buf, n, t, i).start()
        core_copy(buf, n, t).start()

    def spread_relay(buf, n):
        for i in range(1, chips):
            block = lax.rem(chip + i, chips) * 2 + core
            cross_copy(buf, n, block, i).wait_recv()
            core_copy(buf, n, block).start()

    def spread_wait(buf, n):
        for j in range(chips):
            core_copy(buf, n, j * 2 + 1 - core).wait_recv()

    def spread_done(buf, n):
        for i in range(1, chips):
            cross_copy(buf, n, t, i).wait_send()
        for j in range(chips):
            core_copy(buf, n, j * 2 + core).wait_send()

    def stat_copy(l, i, block):
        return pltpu.make_async_remote_copy(
            src_ref=stat_rows.at[l, block], dst_ref=stat_rows.at[l, block],
            send_sem=stat_send.at[l, i], recv_sem=stat_recv.at[l, block],
            device_id={"tp": lax.rem(t + i, tp)}, device_id_type=MESH,
        )

    def halo_copy(l):
        return pltpu.make_async_remote_copy(
            src_ref=tail.at[l], dst_ref=halo.at[l],
            send_sem=halo_send.at[l], recv_sem=halo_recv.at[l],
            device_id={"sp": s + 1}, device_id_type=MESH,
        )

    def normalise(l):
        part = width // tp

        def body(c, carry):
            at = pl.ds(pl.multiple_of(c * CHUNK, CHUNK), CHUNK)
            total = jnp.zeros((CHUNK, 1), F32)
            for b in range(tp):
                x = feats[l, b, at, :].astype(F32)
                total = total + jnp.sum(x * x, axis=1, keepdims=True)
                scaled_feats[b, at, :] = (
                    x * gain[l : l + 1, b * part : (b + 1) * part].astype(F32)
                ).astype(BF16)
            inv[at, :] = jnp.broadcast_to(lax.rsqrt(total / width + EPS), (CHUNK, 128))
            return carry

        lax.fori_loop(0, rows // CHUNK, body, 0)

    local = channels // tp

    def project(l):
        for k, acc in ((SIG, acc_sig), (GATE, acc_gate)):
            def body(b, carry, k=k, acc=acc):
                w = banks[k][l, pl.ds(b * share, share)].reshape(width // tp, local)
                acc[...] += jnp.dot(scaled_feats[b], w, preferred_element_type=F32)
                return carry

            acc[...] = jnp.zeros_like(acc)
            lax.fori_loop(0, tp, body, 0)

        def blend(c, carry):
            at = pl.ds(pl.multiple_of(c * CHUNK, CHUNK), CHUNK)
            r = inv[at, 0:1]
            v = (acc_sig[at, :] * r) * sigmoid(acc_gate[at, :] * r)
            to = pl.ds(pl.multiple_of(hp + c * CHUNK, 8), CHUNK)
            padded[to, :] = v.astype(BF16).astype(F32)
            return carry

        lax.fori_loop(0, rows // CHUNK, blend, 0)
        tail[l] = padded[rows : rows + hp, :].astype(BF16)

        @pl.when(s < sp - 1)
        def _():
            halo_copy(l).start()

    def convolve(l):
        @pl.when(s > 0)
        def _():
            halo_copy(l).wait_recv()
            padded[0:hp, :] = halo[l].astype(F32)

        @pl.when(s == 0)
        def _():
            padded[0:hp, :] = jnp.zeros((hp, local), F32)

        tap_rows = taps[l].astype(F32)
        first = hp - (kernel_taps - 1)
        lane = lax.broadcasted_iota(jnp.int32, (CHUNK, 128), 1)
        for c in range(rows // CHUNK):
            low = c * CHUNK
            total = jnp.broadcast_to(bias[l : l + 1, :].astype(F32), (CHUNK, local))
            for j in range(kernel_taps):
                start = low + first + j
                total = total + tap_rows[j : j + 1, :] * padded[start : start + CHUNK, :]
            filt[low : low + CHUNK, :] = total
            one = jnp.sum(total, axis=1, keepdims=True)
            two = jnp.sum(total * total, axis=1, keepdims=True)
            stat_cols[low : low + CHUNK, :] = jnp.where(
                lane == 0, one, jnp.where(lane == 1, two, 0.0)
            )
        stat_rows[l, t] = jnp.transpose(stat_cols[...])[0:8, :]
        for i in range(1, tp):
            stat_copy(l, i, t).start()

    def activate(l):
        for i in range(1, tp):
            stat_copy(l, i, lax.rem(t + i, tp)).wait_recv()
        sums = jnp.sum(stat_rows[l], axis=0)
        stat_cols[...] = jnp.transpose(
            jnp.concatenate([sums, jnp.zeros((120, rows), F32)], axis=0)
        )
        gains, shifts = ln_gain[l : l + 1, :].astype(F32), ln_shift[l : l + 1, :].astype(F32)

        def body(c, carry):
            at = pl.ds(pl.multiple_of(c * CHUNK, CHUNK), CHUNK)
            average = stat_cols[at, 0:1] / channels
            spread = stat_cols[at, 1:2] / channels - average * average
            v = (filt[at, :] - average) * lax.rsqrt(spread + EPS) * gains + shifts
            acts[l, t, at, :] = (v * sigmoid(v)).astype(BF16)
            return carry

        lax.fori_loop(0, rows // CHUNK, body, 0)

    def update(l):
        columns = width // tp
        tile = min(256, columns)
        deep = 128

        def body(c, carry):
            at = pl.ds(pl.multiple_of(c * deep, deep), deep)
            for n in range(columns // tile):
                cut = slice(n * tile, (n + 1) * tile)
                total = feats[l, t, at, cut].astype(F32)
                for b in range(tp):
                    w = out_all[l, b * share : (b + 1) * share, :, :, cut].reshape(local, tile)
                    total = total + jnp.dot(acts[l, b, at, :], w, preferred_element_type=F32)
                if l + 1 < layers:
                    feats[l + 1, t, at, cut] = total.astype(BF16)
                else:
                    result[at, cut] = total.astype(BF16)
            return carry

        lax.fori_loop(0, rows // deep, body, 0)

    hops = range(sp - 1)
    own(0, SIG)
    own(0, GATE)
    own_stream.wait()
    spread_start(feats.at[0], 0)
    for l in range(layers):
        x_cut = [(d, k) for d in hops for k in (SIG, GATE)]
        middle = len(x_cut) - 3 if l == 0 else len(x_cut) - 2
        for i, (d, k) in enumerate(x_cut):
            if l and i == 0:
                continue
            if i == middle:
                spread_relay(feats.at[l], 2 * l)
            relay(l, k, d)
        own(l, OUT)
        spread_wait(feats.at[l], 2 * l)
        normalise(l)
        for d, k in x_cut:
            other_half(l, k, d)
        project(l)
        relay(l, OUT, 0)
        convolve(l)
        for d in hops[1:]:
            relay(l, OUT, d)
        if l + 1 < layers:
            own(l + 1, SIG)
            own(l + 1, GATE)
        activate(l)
        spread_start(acts.at[l], 2 * l + 1)
        if l + 1 < layers:
            relay(l + 1, SIG, 0)
        spread_relay(acts.at[l], 2 * l + 1)
        for d in hops:
            other_half(l, OUT, d)
        spread_wait(acts.at[l], 2 * l + 1)
        update(l)
        if l + 1 < layers:
            spread_start(feats.at[l + 1], 2 * l + 2)

    for l in range(layers):
        for k in (SIG, GATE, OUT):
            own(l, k, done=True)
            for d in hops:
                relay(l, k, d, done=True)
        spread_done(feats.at[l], 2 * l)
        spread_done(acts.at[l], 2 * l + 1)
        for i in range(1, tp):
            stat_copy(l, i, t).wait_send()

        @pl.when(s < sp - 1)
        def _(l=l):
            halo_copy(l).wait_send()


def shards(counts, stream, norm_gain, w_signal, w_gate, conv_taps, conv_bias, ln_gain, ln_shift, w_out):
    groups, sp, tp = counts
    layers, deep, local = w_signal.shape
    rows, part = stream.shape
    kernel_taps = conv_taps.shape[1]
    hp = -(-(kernel_taps - 1) // 16) * 16
    width, channels = part * tp, local * tp
    halves = lambda w: w.reshape(layers, groups, w.shape[1] // groups, w.shape[2])
    bank = lambda w: pltpu.VMEM((layers, sp, groups, w.shape[1] // groups, w.shape[2]), BF16)
    dma = lambda *shape: pltpu.SemaphoreType.DMA(shape)
    anywhere = pl.BlockSpec(memory_space=pl.ANY)
    inside = pl.BlockSpec(memory_space=pltpu.VMEM)
    return pl.pallas_call(
        functools.partial(
            kernel, (groups, sp, tp, layers, rows, kernel_taps, hp, width, channels)
        ),
        out_shape=jax.ShapeDtypeStruct(stream.shape, BF16),
        in_specs=[anywhere, inside, anywhere, anywhere, inside, inside, inside, inside, anywhere],
        out_specs=inside,
        scratch_shapes=[
            bank(w_signal), bank(w_gate), bank(w_out),
            pltpu.VMEM((layers, tp, rows, part), BF16),
            pltpu.VMEM((tp, rows, part), BF16),
            pltpu.VMEM((rows, 128), F32),
            pltpu.VMEM((rows, local), F32),
            pltpu.VMEM((rows, local), F32),
            pltpu.VMEM((layers, hp, local), BF16),
            pltpu.VMEM((layers, hp, local), BF16),
            pltpu.VMEM((hp + rows, local), F32),
            pltpu.VMEM((rows, local), F32),
            pltpu.VMEM((rows, 128), F32),
            pltpu.VMEM((layers, tp, 8, rows), F32),
            pltpu.VMEM((layers, tp, rows, local), BF16),
            dma(layers, 3), pltpu.SemaphoreType.DMA,
            dma(layers, 3, 2, sp), dma(layers, 3, sp), dma(layers, 3, sp), dma(layers, 3, sp),
            dma(2 * layers, tp), dma(2 * layers, tp), dma(2 * layers, tp), dma(2 * layers, tp),
            dma(layers), dma(layers), dma(layers, tp), dma(layers, tp),
        ],
        compiler_params=pltpu.CompilerParams(
            collective_id=0, has_side_effects=True, vmem_limit_bytes=60 * 1024 * 1024
        ),
    )(
        stream, norm_gain, halves(w_signal), halves(w_gate), conv_taps, conv_bias,
        ln_gain, ln_shift, halves(w_out),
    )


def solution(mesh):
    counts = tuple(mesh.shape[name] for name in ("grp", "sp", "tp"))
    return jax.shard_map(
        functools.partial(shards, counts),
        mesh=mesh,
        in_specs=(
            P(("grp", "sp"), "tp"),
            P(),
            P(None, "sp", "tp"),
            P(None, "sp", "tp"),
            P(None, None, "tp"),
            P(None, "tp"),
            P(None, "tp"),
            P(None, "tp"),
            P(None, "sp", "tp"),
        ),
        out_specs=P(("grp", "sp"), "tp"),
        check_vma=False,
    )
```

time: 355 us -> 139 us (0.39)
  waiting for transfers between devices: 275 us -> 0 us
  Pallas kernels: 0 us -> 135 us
  blocking collectives: 28.5 us -> 0 us
  matrix products: 19.1 us -> 0 us
  between operations: 13.3 us -> 0.01 us
  other arithmetic: 12.7 us -> 0 us
  starting transfers between devices: 4.83 us -> 0 us
    all_gather x5 -> x0, waiting for transfers between devices: 269 us -> none  [the longest x1 79.8 us: shards(): lax.all_gather(w_gate, 'sp', axis=1, tiled=True)]
    pallas_call x0 -> x1, Pallas kernels: none -> 135 us  [shards(): pl.pallas_call(functools.partial(kernel, (groups, sp, tp, layers, rows, k...]
    dot_general x6 -> x0, matrix products: 19.1 us -> none  [product(): return jnp.dot(left, right, preferred_element_type=jnp.float32)]
    all_gather x2 -> x0, blocking collectives: 16.7 us -> none  [shards(): channels = lax.all_gather(activated, 'tp', axis=1, tiled=True)]
    psum x2 -> x0, blocking collectives: 11.8 us -> none  [shards(): lax.psum((jnp.sum(filtered, axis=-1), jnp.sum(filtered * filtered, axis=-...]
    reduce_sum x4 -> x0, other arithmetic: 8.95 us -> none  [the longest x2 5.16 us: shards(): jnp.mean(widened * widened, axis=-1, keepdims=True) + EPS]
    ppermute x2 -> x0, starting transfers between devices: 4.68 us -> none  [shifted(): lax.ppermute(value, axis, [(source, source + steps) for source in range(i...]
  transfers between devices with their start and end apart: 7 -> 0, of which waited for: 7 -> 0; matrix products, arithmetic and copies ran while one was open for 4% -> 0% of each run, Pallas kernels for 0% -> 0%
where the time goes in v1:
time: 139 us; the launch traced here: 138 us
  Pallas kernels  135 us (97%)
  local copies, waits for them, and re-layouts  3.44 us (2%)
    pallas_call x1, Pallas kernels, shards(): pl.pallas_call(functools.partial(kernel, (groups, sp, tp, layers, rows, k...  135 us
    unnamed x2, local copies, waits for them, and re-layouts  3.44 us

profile of v1, /device:TPU:0, one launch (start us, length us, event | category | flops | bytes accessed | tf_op | source)
XLA Modules:
  0.0 138.1 jit_solution(10330780233313512829)
XLA Ops:
  0.0 1.4 copy.10.taps
  1.4 134.7 %shard_map.91 = bf16[384,1024]{1,0:T(8,128)(2,1)} custom-call(bf16[384,1024]{1,0:T(8,128)(2,1)} %stream.1, bf16[2,4096]{1,0:T(2,128)(2,1)} %gain.1, bf16[2,2,512,256]{3,2,1,0:T(8,128)(2,1)} %bitcast.3, bf16[2,2,512,256]{3,2,1,0:T(8,128)(2,1)} %bitcast.4, bf16[2,31,256]{2,1,0:T(8,128)(2,1)} %copy.10.taps, bf16[2,256]{1,0:T(2,128)(2,1)} %bias.1, ...), custom_call_target="tpu_custom_call" | custom-call | tf_op jit(solution)/shard_map/pallas_call | solution.py:354
  136.1 2.1 %copy.12 = bf16[384,1024]{1,0:T(8,128)(2,1)} copy(bf16[384,1024]{1,0:T(8,128)(2,1)} %shard_map.91) | data formatting | bytes 1572864

commit v2 on v1

--- a/solution.py
+++ b/solution.py
@@ -13,6 +13,7 @@
 BF16 = jnp.bfloat16
 SIG, GATE, OUT = 0, 1, 2
 CHUNK = 32
+PIECES = 2
 
 
 def sigmoid(v):
@@ -25,7 +26,7 @@
     result,
     sig_all, gate_all, out_all, feats, scaled_feats, inv, acc_sig, acc_gate,
     tail, halo, padded, filt, stat_cols, stat_rows, acts,
-    load_sem, stream_sem, z_send, z_recv, y_send, y_recv,
+    load_sem, stream_sem, own_send, z_send, z_recv, y_send, y_recv,
     cross_send, cross_recv, core_send, core_recv,
     halo_send, halo_recv, stat_send, stat_recv,
 ):
@@ -38,6 +39,9 @@
     banks = (sig_all, gate_all, out_all)
     held = (w_signal, w_gate, w_out)
 
+    inner = (s > 0) & (s < sp - 1)
+    pieces = [w.shape[2] for w in held]
+
     def load(l, k):
         return pltpu.make_async_copy(held[k].at[l], banks[k].at[l, s], load_sem.at[l, k])
 
@@ -69,57 +73,71 @@
         jnp.where(s > 0, 1, 0) + jnp.where(s < sp - 1, 1, 0) + (groups - 1 + tp - 1),
     )
 
-    def z_copy(l, k, shard, way):
-        ref = banks[k].at[l, shard, g]
+    def z_copy(l, k, q, shard, way, mine=False):
+        ref = banks[k].at[l, shard, g, q]
         return pltpu.make_async_remote_copy(
             src_ref=ref, dst_ref=ref,
-            send_sem=z_send.at[l, k, way, shard], recv_sem=z_recv.at[l, k, shard],
+            send_sem=own_send.at[l, k, q] if mine and way else z_send.at[l, k, q, shard],
+            recv_sem=z_recv.at[l, k, q, shard],
             device_id={"sp": s + 1 if way == 0 else s - 1}, device_id_type=MESH,
         )
 
-    def y_copy(l, k, shard):
-        ref = banks[k].at[l, shard, g]
+    def y_copy(l, k, q, shard, half, where):
+        ref = banks[k].at[l, shard, half, q]
         return pltpu.make_async_remote_copy(
             src_ref=ref, dst_ref=ref,
-            send_sem=y_send.at[l, k, shard], recv_sem=y_recv.at[l, k, shard],
-            device_id={"grp": 1 - g}, device_id_type=MESH,
+            send_sem=y_send.at[l, k, q, shard], recv_sem=y_recv.at[l, k, q, shard],
+            device_id=where, device_id_type=MESH,
         )
 
     def own(l, k, done=False):
         if not done:
             load(l, k).wait()
-        for way, there in ((0, s < sp - 1), (1, s > 0)):
+        for way, there, end in ((0, s < sp - 1, s == 0), (1, s > 0, s == sp - 1)):
             @pl.when(there)
-            def _(way=way):
-                copy = z_copy(l, k, s, way)
-                copy.wait_send() if done else copy.start()
+            def _(way=way, end=end):
+                for q in range(pieces[k]):
+                    copy = z_copy(l, k, q, s, way, True)
+                    copy.wait_send() if done else copy.start()
+
+                @pl.when(end)
+                def _():
+                    for q in range(pieces[k]):
+                        where = {"sp": s + 1 if way == 0 else s - 1}
+                        copy = y_copy(l, k, q, s, 1 - g, where)
+                        copy.wait_send() if done else copy.start()
 
     def sides(d):
+        left, right = s - 1 - d, s + 1 + d
         return (
-            (0, s - 1 - d, s - 1 - d >= 0, s < sp - 1),
-            (1, s + 1 + d, s + 1 + d <= sp - 1, s > 0),
+            (0, left, left >= 0, s < sp - 1, (left > 0) | (d > 0)),
+            (1, right, right <= sp - 1, s > 0, (right < sp - 1) | (d > 0)),
         )
 
     def relay(l, k, d, done=False):
-        for way, shard, here, onward in sides(d):
+        for way, shard, here, onward, across in sides(d):
             @pl.when(here)
-            def _(way=way, shard=shard, onward=onward):
-                if not done:
-                    z_copy(l, k, shard, way).wait_recv()
-
-                @pl.when(onward)
-                def _():
-                    copy = z_copy(l, k, shard, way)
-                    copy.wait_send() if done else copy.start()
-
-                copy = y_copy(l, k, shard)
-                copy.wait_send() if done else copy.start()
+            def _(way=way, shard=shard, onward=onward, across=across):
+                for q in range(pieces[k]):
+                    if not done:
+                        z_copy(l, k, q, shard, way).wait_recv()
+
+                    @pl.when(onward)
+                    def _():
+                        copy = z_copy(l, k, q, shard, way)
+                        copy.wait_send() if done else copy.start()
+
+                    @pl.when(across)
+                    def _():
+                        copy = y_copy(l, k, q, shard, g, {"grp": 1 - g})
+                        copy.wait_send() if done else copy.start()
 
     def other_half(l, k, d):
-        for _, shard, here, _ in sides(d):
+        for _, shard, here, _, _ in sides(d):
             @pl.when(here)
             def _(shard=shard):
-                y_copy(l, k, shard).wait_recv()
+                for q in range(pieces[k]):
+                    y_copy(l, k, q, shard, 1 - g, {"grp": 1 - g}).wait_recv()
 
     def cross_copy(buf, n, block, i):
         ref = buf.at[block]
@@ -217,19 +235,22 @@
             halo_copy(l).start()
 
     def convolve(l):
-        @pl.when(s > 0)
-        def _():
-            halo_copy(l).wait_recv()
-            padded[0:hp, :] = halo[l].astype(F32)
-
-        @pl.when(s == 0)
-        def _():
-            padded[0:hp, :] = jnp.zeros((hp, local), F32)
-
-        tap_rows = taps[l].astype(F32)
+        def settle():
+            @pl.when(s > 0)
+            def _():
+                halo_copy(l).wait_recv()
+                padded[0:hp, :] = halo[l].astype(F32)
+
+            @pl.when(s == 0)
+            def _():
+                padded[0:hp, :] = jnp.zeros((hp, local), F32)
+
+        tap_rows = taps[:, l, :].astype(F32)
         first = hp - (kernel_taps - 1)
         lane = lax.broadcasted_iota(jnp.int32, (CHUNK, 128), 1)
-        for c in range(rows // CHUNK):
+        for c in [*range(1, rows // CHUNK), 0]:
+            if c == 0:
+                settle()
             low = c * CHUNK
             total = jnp.broadcast_to(bias[l : l + 1, :].astype(F32), (CHUNK, local))
             for j in range(kernel_taps):
@@ -275,7 +296,7 @@
                 cut = slice(n * tile, (n + 1) * tile)
                 total = feats[l, t, at, cut].astype(F32)
                 for b in range(tp):
-                    w = out_all[l, b * share : (b + 1) * share, :, :, cut].reshape(local, tile)
+                    w = out_all[l, b * share : (b + 1) * share, :, :, :, cut].reshape(local, tile)
                     total = total + jnp.dot(acts[l, b, at, :], w, preferred_element_type=F32)
                 if l + 1 < layers:
                     feats[l + 1, t, at, cut] = total.astype(BF16)
@@ -297,21 +318,33 @@
             if l and i == 0:
                 continue
             if i == middle:
+                if l:
+                    own(l, OUT)
                 spread_relay(feats.at[l], 2 * l)
             relay(l, k, d)
-        own(l, OUT)
+        if l == 0:
+            own(l, OUT)
         spread_wait(feats.at[l], 2 * l)
         normalise(l)
         for d, k in x_cut:
             other_half(l, k, d)
         project(l)
-        relay(l, OUT, 0)
-        convolve(l)
-        for d in hops[1:]:
-            relay(l, OUT, d)
+
+        @pl.when(inner)
+        def _(l=l):
+            for d in hops:
+                relay(l, OUT, d)
+
         if l + 1 < layers:
             own(l + 1, SIG)
             own(l + 1, GATE)
+        convolve(l)
+
+        @pl.when(jnp.logical_not(inner))
+        def _(l=l):
+            for d in hops:
+                relay(l, OUT, d)
+
         activate(l)
         spread_start(acts.at[l], 2 * l + 1)
         if l + 1 < layers:
@@ -346,8 +379,16 @@
     kernel_taps = conv_taps.shape[1]
     hp = -(-(kernel_taps - 1) // 16) * 16
     width, channels = part * tp, local * tp
-    halves = lambda w: w.reshape(layers, groups, w.shape[1] // groups, w.shape[2])
-    bank = lambda w: pltpu.VMEM((layers, sp, groups, w.shape[1] // groups, w.shape[2]), BF16)
+
+    def cut(w):
+        half = w.shape[1] // groups
+        count = PIECES if half % (16 * PIECES) == 0 else 1
+        return w.reshape(layers, groups, count, half // count, w.shape[2])
+
+    w_signal, w_gate, w_out = cut(w_signal), cut(w_gate), cut(w_out)
+    bank = lambda w: pltpu.VMEM((layers, sp) + w.shape[1:], BF16)
+    most = max(w.shape[2] for w in (w_signal, w_gate, w_out))
+    line = (layers, 3, most, sp)
     dma = lambda *shape: pltpu.SemaphoreType.DMA(shape)
     anywhere = pl.BlockSpec(memory_space=pl.ANY)
     inside = pl.BlockSpec(memory_space=pltpu.VMEM)
@@ -373,7 +414,7 @@
             pltpu.VMEM((layers, tp, 8, rows), F32),
             pltpu.VMEM((layers, tp, rows, local), BF16),
             dma(layers, 3), pltpu.SemaphoreType.DMA,
-            dma(layers, 3, 2, sp), dma(layers, 3, sp), dma(layers, 3, sp), dma(layers, 3, sp),
+            dma(layers, 3, most), dma(*line), dma(*line), dma(*line), dma(*line),
             dma(2 * layers, tp), dma(2 * layers, tp), dma(2 * layers, tp), dma(2 * layers, tp),
             dma(layers), dma(layers), dma(layers, tp), dma(layers, tp),
         ],
@@ -381,8 +422,8 @@
             collective_id=0, has_side_effects=True, vmem_limit_bytes=60 * 1024 * 1024
         ),
     )(
-        stream, norm_gain, halves(w_signal), halves(w_gate), conv_taps, conv_bias,
-        ln_gain, ln_shift, halves(w_out),
+        stream, norm_gain, w_signal, w_gate, jnp.transpose(conv_taps, (1, 0, 2)), conv_bias,
+        ln_gain, ln_shift, w_out,
     )
 
 

time: 139 us -> 137 us (0.986)
    unnamed x2 -> x1, local copies, waits for them, and re-layouts: 3.44 us -> 2.06 us
where the time goes in v2:
time: 137 us
  Pallas kernels  135 us (99%)
  local copies, waits for them, and re-layouts  2.06 us (2%)
    pallas_call x1, Pallas kernels, shards(): pl.pallas_call(functools.partial(kernel, (groups, sp, tp, layers, rows, k...  135 us

profile of v2, /device:TPU:0, one launch (start us, length us, event | category | flops | bytes accessed | tf_op | source)
XLA Modules:
  0.0 136.8 jit_solution(3390856205807124957)
XLA Ops:
  0.0 134.7 %shard_map.91 = bf16[384,1024]{1,0:T(8,128)(2,1)} custom-call(bf16[384,1024]{1,0:T(8,128)(2,1)} %stream.1, bf16[2,4096]{1,0:T(2,128)(2,1)} %gain.1, bf16[2,2,2,256,256]{4,3,2,1,0:T(8,128)(2,1)} %bitcast.4, bf16[2,2,2,256,256]{4,3,2,1,0:T(8,128)(2,1)} %bitcast.5, bf16[31,2,256]{2,1,0:T(2,128)(2,1)} %bitcast.7, bf16[2,256]{1,0:T(2,128)(2,1)} %bias.1, ...), custom_call_target="tpu_custom_call" | custom-call | tf_op jit(solution)/shard_map/pallas_call | solution.py:395
  134.7 2.1 %copy.11 = bf16[384,1024]{1,0:T(8,128)(2,1)} copy(bf16[384,1024]{1,0:T(8,128)(2,1)} %shard_map.91) | data formatting | bytes 1572864

commit v3 on v2

--- a/solution.py
+++ b/solution.py
@@ -26,6 +26,7 @@
     result,
     sig_all, gate_all, out_all, feats, scaled_feats, inv, acc_sig, acc_gate,
     tail, halo, padded, filt, stat_cols, stat_rows, acts,
+    guest, sent, got, guest_sems,
     load_sem, stream_sem, own_send, z_send, z_recv, y_send, y_recv,
     cross_send, cross_recv, core_send, core_recv,
     halo_send, halo_recv, stat_send, stat_recv,
@@ -40,6 +41,10 @@
     held = (w_signal, w_gate, w_out)
 
     inner = (s > 0) & (s < sp - 1)
+    end = jnp.logical_not(inner)
+    host = (s == 1) | (s == sp - 2)
+    inward = jnp.where(s == 0, 1, sp - 2)
+    outward = jnp.where(s == 1, 0, sp - 1)
     pieces = [w.shape[2] for w in held]
 
     def load(l, k):
@@ -90,32 +95,46 @@
             device_id=where, device_id_type=MESH,
         )
 
+    def hosted(l, k):
+        return l == 0 and k != OUT
+
     def own(l, k, done=False):
         if not done:
             load(l, k).wait()
-        for way, there, end in ((0, s < sp - 1, s == 0), (1, s > 0, s == sp - 1)):
+        spare = 1 if hosted(l, k) else 0
+        for way, there, last in (
+            (0, s < sp - 1 - spare, s == 0), (1, s > spare, s == sp - 1)
+        ):
             @pl.when(there)
-            def _(way=way, end=end):
+            def _(way=way, last=last):
                 for q in range(pieces[k]):
                     copy = z_copy(l, k, q, s, way, True)
                     copy.wait_send() if done else copy.start()
 
-                @pl.when(end)
+                if spare:
+                    return
+
+                @pl.when(last)
                 def _():
                     for q in range(pieces[k]):
                         where = {"sp": s + 1 if way == 0 else s - 1}
                         copy = y_copy(l, k, q, s, 1 - g, where)
                         copy.wait_send() if done else copy.start()
 
-    def sides(d):
+    def sides(l, k, d):
         left, right = s - 1 - d, s + 1 + d
+        if hosted(l, k):
+            return (
+                (0, left, (left >= 0) & inner, s < sp - 2, left >= 0),
+                (1, right, (right <= sp - 1) & inner, s > 1, right <= sp - 1),
+            )
         return (
             (0, left, left >= 0, s < sp - 1, (left > 0) | (d > 0)),
             (1, right, right <= sp - 1, s > 0, (right < sp - 1) | (d > 0)),
         )
 
     def relay(l, k, d, done=False):
-        for way, shard, here, onward, across in sides(d):
+        for way, shard, here, onward, across in sides(l, k, d):
             @pl.when(here)
             def _(way=way, shard=shard, onward=onward, across=across):
                 for q in range(pieces[k]):
@@ -133,7 +152,7 @@
                         copy.wait_send() if done else copy.start()
 
     def other_half(l, k, d):
-        for _, shard, here, _, _ in sides(d):
+        for _, shard, here, _, _ in sides(l, k, d):
             @pl.when(here)
             def _(shard=shard):
                 for q in range(pieces[k]):
@@ -183,6 +202,9 @@
             device_id={"tp": lax.rem(t + i, tp)}, device_id_type=MESH,
         )
 
+    def tail_goes(l):
+        return inner if l == 0 else s < sp - 1
+
     def halo_copy(l):
         return pltpu.make_async_remote_copy(
             src_ref=tail.at[l], dst_ref=halo.at[l],
@@ -190,14 +212,28 @@
             device_id={"sp": s + 1}, device_id_type=MESH,
         )
 
-    def normalise(l):
+    def guest_copy():
+        return pltpu.make_async_remote_copy(
+            src_ref=feats.at[0, t], dst_ref=guest.at[t],
+            send_sem=guest_sems.at[0], recv_sem=guest_sems.at[1],
+            device_id={"sp": inward}, device_id_type=MESH,
+        )
+
+    def back_copy():
+        return pltpu.make_async_remote_copy(
+            src_ref=sent, dst_ref=got,
+            send_sem=guest_sems.at[2], recv_sem=guest_sems.at[3],
+            device_id={"sp": outward}, device_id_type=MESH,
+        )
+
+    def normalise(l, source):
         part = width // tp
 
         def body(c, carry):
             at = pl.ds(pl.multiple_of(c * CHUNK, CHUNK), CHUNK)
             total = jnp.zeros((CHUNK, 1), F32)
             for b in range(tp):
-                x = feats[l, b, at, :].astype(F32)
+                x = source[b, at, :].astype(F32)
                 total = total + jnp.sum(x * x, axis=1, keepdims=True)
                 scaled_feats[b, at, :] = (
                     x * gain[l : l + 1, b * part : (b + 1) * part].astype(F32)
@@ -209,7 +245,7 @@
 
     local = channels // tp
 
-    def project(l):
+    def project(l, visiting=False):
         for k, acc in ((SIG, acc_sig), (GATE, acc_gate)):
             def body(b, carry, k=k, acc=acc):
                 w = banks[k][l, pl.ds(b * share, share)].reshape(width // tp, local)
@@ -224,22 +260,31 @@
             r = inv[at, 0:1]
             v = (acc_sig[at, :] * r) * sigmoid(acc_gate[at, :] * r)
             to = pl.ds(pl.multiple_of(hp + c * CHUNK, 8), CHUNK)
-            padded[to, :] = v.astype(BF16).astype(F32)
+            if visiting:
+                sent[at, :] = v.astype(BF16)
+            else:
+                padded[to, :] = v.astype(BF16).astype(F32)
             return carry
 
         lax.fori_loop(0, rows // CHUNK, blend, 0)
-        tail[l] = padded[rows : rows + hp, :].astype(BF16)
-
-        @pl.when(s < sp - 1)
-        def _():
-            halo_copy(l).start()
+        if not visiting:
+            tail[l] = padded[rows : rows + hp, :].astype(BF16)
+
+            @pl.when(tail_goes(l))
+            def _():
+                halo_copy(l).start()
 
     def convolve(l):
         def settle():
-            @pl.when(s > 0)
+            @pl.when(s > (1 if l == 0 else 0))
             def _():
                 halo_copy(l).wait_recv()
                 padded[0:hp, :] = halo[l].astype(F32)
+
+            if l == 0:
+                @pl.when(s == 1)
+                def _():
+                    padded[0:hp, :] = sent[rows - hp : rows, :].astype(F32)
 
             @pl.when(s == 0)
             def _():
@@ -307,67 +352,131 @@
         lax.fori_loop(0, rows // deep, body, 0)
 
     hops = range(sp - 1)
-    own(0, SIG)
-    own(0, GATE)
-    own_stream.wait()
-    spread_start(feats.at[0], 0)
-    for l in range(layers):
-        x_cut = [(d, k) for d in hops for k in (SIG, GATE)]
-        middle = len(x_cut) - 3 if l == 0 else len(x_cut) - 2
-        for i, (d, k) in enumerate(x_cut):
-            if l and i == 0:
-                continue
-            if i == middle:
-                if l:
-                    own(l, OUT)
-                spread_relay(feats.at[l], 2 * l)
-            relay(l, k, d)
-        if l == 0:
-            own(l, OUT)
-        spread_wait(feats.at[l], 2 * l)
-        normalise(l)
-        for d, k in x_cut:
-            other_half(l, k, d)
-        project(l)
-
-        @pl.when(inner)
-        def _(l=l):
-            for d in hops:
-                relay(l, OUT, d)
-
+    cuts = [(d, k) for d in hops for k in (SIG, GATE)]
+    visit = 2 * layers
+
+    def ahead(l):
         if l + 1 < layers:
             own(l + 1, SIG)
             own(l + 1, GATE)
+
+    own_stream.wait()
+
+    @pl.when(end)
+    def _():
+        guest_copy().start()
+
+    own(0, SIG)
+    own(0, GATE)
+
+    @pl.when(inner)
+    def _():
+        spread_start(feats.at[0], 0)
+
+    for i, (d, k) in enumerate(cuts):
+        relay(0, k, d)
+        if i == 1:
+            own(0, OUT)
+
+            @pl.when(host)
+            def _():
+                guest_copy().wait_recv()
+                spread_start(guest, visit)
+
+    @pl.when(inner)
+    def _():
+        spread_relay(feats.at[0], 0)
+        spread_wait(feats.at[0], 0)
+
+    for d, k in cuts:
+        other_half(0, k, d)
+
+    @pl.when(host)
+    def _():
+        spread_relay(guest, visit)
+        spread_wait(guest, visit)
+        normalise(0, guest)
+        project(0, True)
+        back_copy().start()
+
+    for d in hops:
+        relay(0, OUT, d)
+    ahead(0)
+
+    @pl.when(inner)
+    def _():
+        normalise(0, feats.at[0])
+        project(0)
+
+    @pl.when(end)
+    def _():
+        back_copy().wait_recv()
+        padded[hp : hp + rows, :] = got[...].astype(F32)
+
+    for l in range(layers):
+        if l:
+            for d, k in cuts[3:]:
+                relay(l, k, d)
+            own(l, OUT)
+            spread_relay(feats.at[l], 2 * l)
+            spread_wait(feats.at[l], 2 * l)
+            normalise(l, feats.at[l])
+            for d, k in cuts:
+                other_half(l, k, d)
+            project(l)
+
+            @pl.when(inner)
+            def _(l=l):
+                for d in hops:
+                    relay(l, OUT, d)
+
+            ahead(l)
         convolve(l)
-
-        @pl.when(jnp.logical_not(inner))
-        def _(l=l):
-            for d in hops:
-                relay(l, OUT, d)
-
+        if l:
+            @pl.when(end)
+            def _(l=l):
+                for d in hops:
+                    relay(l, OUT, d)
+
+        more = l + 1 < layers
+        if more:
+            relay(l + 1, cuts[0][1], cuts[0][0])
         activate(l)
         spread_start(acts.at[l], 2 * l + 1)
-        if l + 1 < layers:
-            relay(l + 1, SIG, 0)
+        if more:
+            relay(l + 1, cuts[1][1], cuts[1][0])
         spread_relay(acts.at[l], 2 * l + 1)
         for d in hops:
             other_half(l, OUT, d)
         spread_wait(acts.at[l], 2 * l + 1)
         update(l)
-        if l + 1 < layers:
+        if more:
             spread_start(feats.at[l + 1], 2 * l + 2)
+            relay(l + 1, cuts[2][1], cuts[2][0])
+
+    @pl.when(end)
+    def _():
+        guest_copy().wait_send()
+
+    @pl.when(host)
+    def _():
+        back_copy().wait_send()
+        spread_done(guest, visit)
 
     for l in range(layers):
         for k in (SIG, GATE, OUT):
             own(l, k, done=True)
             for d in hops:
                 relay(l, k, d, done=True)
-        spread_done(feats.at[l], 2 * l)
+        @pl.when(inner if l == 0 else s >= 0)
+        def _(l=l):
+            spread_done(feats.at[l], 2 * l)
+
         spread_done(acts.at[l], 2 * l + 1)
         for i in range(1, tp):
             stat_copy(l, i, t).wait_send()
 
-        @pl.when(s < sp - 1)
+        @pl.when(tail_goes(l))
         def _(l=l):
             halo_copy(l).wait_send()
 
@@ -413,9 +522,14 @@
             pltpu.VMEM((rows, 128), F32),
             pltpu.VMEM((layers, tp, 8, rows), F32),
             pltpu.VMEM((layers, tp, rows, local), BF16),
+            pltpu.VMEM((tp, rows, part), BF16),
+            pltpu.VMEM((rows, local), BF16),
+            pltpu.VMEM((rows, local), BF16),
+            dma(4),
             dma(layers, 3), pltpu.SemaphoreType.DMA,
             dma(layers, 3, most), dma(*line), dma(*line), dma(*line), dma(*line),
-            dma(2 * layers, tp), dma(2 * layers, tp), dma(2 * layers, tp), dma(2 * layers, tp),
+            dma(2 * layers + 1, tp), dma(2 * layers + 1, tp),
+            dma(2 * layers + 1, tp), dma(2 * layers + 1, tp),
             dma(layers), dma(layers), dma(layers, tp), dma(layers, tp),
         ],
         compiler_params=pltpu.CompilerParams(

time: 137 us -> 163 us (1.19)
  Pallas kernels: 135 us -> 161 us
    pallas_call x1, Pallas kernels: 135 us -> 161 us  [shards(): pl.pallas_call(functools.partial(kernel, (groups, sp, tp, layers, rows, k...]
where the time goes in v3:
time: 163 us
  Pallas kernels  161 us (99%)
  local copies, waits for them, and re-layouts  2.06 us (1%)
    pallas_call x1, Pallas kernels, shards(): pl.pallas_call(functools.partial(kernel, (groups, sp, tp, layers, rows, k...  161 us

profile of v3, /device:TPU:0, one launch (start us, length us, event | category | flops | bytes accessed | tf_op | source)
XLA Modules:
  0.0 162.9 jit_solution(6284536596531563162)
XLA Ops:
  0.0 160.8 %shard_map.91 = bf16[384,1024]{1,0:T(8,128)(2,1)} custom-call(bf16[384,1024]{1,0:T(8,128)(2,1)} %stream.1, bf16[2,4096]{1,0:T(2,128)(2,1)} %gain.1, bf16[2,2,2,256,256]{4,3,2,1,0:T(8,128)(2,1)} %bitcast.4, bf16[2,2,2,256,256]{4,3,2,1,0:T(8,128)(2,1)} %bitcast.5, bf16[31,2,256]{2,1,0:T(2,128)(2,1)} %bitcast.7, bf16[2,256]{1,0:T(2,128)(2,1)} %bias.1, ...), custom_call_target="tpu_custom_call" | custom-call | tf_op jit(solution)/shard_map/pallas_call | solution.py:504
  160.9 2.1 %copy.11 = bf16[384,1024]{1,0:T(8,128)(2,1)} copy(bf16[384,1024]{1,0:T(8,128)(2,1)} %shard_map.91) | data formatting | bytes 1572864

commit v4 on v2

--- a/solution.py
+++ b/solution.py
@@ -217,6 +217,8 @@
                 return carry
 
             acc[...] = jnp.zeros_like(acc)
+            for d in range(sp - 1):
+                other_half(l, k, d)
             lax.fori_loop(0, tp, body, 0)
 
         def blend(c, carry):
@@ -326,8 +328,6 @@
             own(l, OUT)
         spread_wait(feats.at[l], 2 * l)
         normalise(l)
-        for d, k in x_cut:
-            other_half(l, k, d)
         project(l)
 
         @pl.when(inner)

time: 137 us -> 136 us (level)
  Pallas kernels: 135 us -> 133 us
where the time goes in v4:
time: 136 us
  Pallas kernels  133 us (98%)
  local copies, waits for them, and re-layouts  2.06 us (2%)
    pallas_call x1, Pallas kernels, shards(): pl.pallas_call(functools.partial(kernel, (groups, sp, tp, layers, rows, k...  133 us

profile of v4, /device:TPU:0, one launch (start us, length us, event | category | flops | bytes accessed | tf_op | source)
XLA Modules:
  0.0 135.5 jit_solution(4683719726377451037)
XLA Ops:
  0.0 133.5 %shard_map.91 = bf16[384,1024]{1,0:T(8,128)(2,1)} custom-call(bf16[384,1024]{1,0:T(8,128)(2,1)} %stream.1, bf16[2,4096]{1,0:T(2,128)(2,1)} %gain.1, bf16[2,2,2,256,256]{4,3,2,1,0:T(8,128)(2,1)} %bitcast.4, bf16[2,2,2,256,256]{4,3,2,1,0:T(8,128)(2,1)} %bitcast.5, bf16[31,2,256]{2,1,0:T(2,128)(2,1)} %bitcast.7, bf16[2,256]{1,0:T(2,128)(2,1)} %bias.1, ...), custom_call_target="tpu_custom_call" | custom-call | tf_op jit(solution)/shard_map/pallas_call | solution.py:395
  133.5 2.1 %copy.11 = bf16[384,1024]{1,0:T(8,128)(2,1)} copy(bf16[384,1024]{1,0:T(8,128)(2,1)} %shard_map.91) | data formatting | bytes 1572864
